TPU v7x, 32 devices: a whole 2x2x4 slice. The times are simulated.
32 devices in a mesh: sp: 4 (over y, x), tp: 8 (over z, core).
Axes of the slice: x: 2, y: 2, z: 4, core: 2. Of those that a mesh axis runs over, the one named last changes fastest.
Arguments:
- conv_outer: bfloat16 [2048, 1024], P('tp', 'sp'), may hold values from -6 to 6
- conv_inner: bfloat16 [2048, 1024], P('tp', 'sp'), may hold values from -6 to 6
- conv_input: bfloat16 [2048, 1024], P('tp', 'sp'), may hold values from -6 to 6
- conv_taps: float32 [3, 2048], P(None, 'tp'), may hold values from -3 to 3
- out_proj: bfloat16 [2048, 4096], P('tp'), may hold values from -0.125 to 0.125
- mixed_state: bfloat16 [1024, 4096], P('sp', 'tp'), may hold values from -6 to 6
- route_ids: int32 [1024, 2], P('sp'), may hold values from 0 to 3, all different within a row; in each aligned block of 256 rows (0 to 255, 256 to 511, ...) at most 256 rows name the same one
- route_weights: float32 [1024, 2], P('sp'), may hold values from 0.1 to 1
- w_gate: bfloat16 [4, 2048, 4096], P('sp', 'tp'), may hold values from -0.09375 to 0.09375
- w_up: bfloat16 [4, 2048, 4096], P('sp', 'tp'), may hold values from -0.09375 to 0.09375
- w_down: bfloat16 [4, 2048, 4096], P('sp', 'tp'), may hold values from -0.125 to 0.125
- cotangent: bfloat16 [1024, 4096], P('sp', 'tp'), may hold values from -8 to 8
Outputs:
- grad_gate: float32 [4, 2048, 4096], P('sp', 'tp')
- grad_up: float32 [4, 2048, 4096], P('sp', 'tp')
- grad_down: float32 [4, 2048, 4096], P('sp', 'tp')
- grad_mixed: bfloat16 [1024, 4096], P('sp', 'tp')
- grad_proj: float32 [2048, 4096], P('tp', 'sp')
- grad_outer: bfloat16 [2048, 1024], P('tp', 'sp')
- grad_inner: bfloat16 [2048, 1024], P('tp', 'sp')
- grad_input: bfloat16 [2048, 1024], P('tp', 'sp')
Inputs may be any that keep to these rules, and one draw needn't show every extreme that they name: `route_ids`: each row names 2 different experts; among the tokens of one index of sp no expert is named more than 256 times, a bound that some block reaches.
All inputs are finite; a program needn't handle non-finite values.
Results may differ from a plain program's by a relative error of at most 0.022.
Values may be sent and summed in bfloat16 or wider, within the bound.
A program may use at most 128 MiB of HBM per device.

v0:
```python
import jax
import jax.numpy as jnp
from jax import lax
from jax.sharding import PartitionSpec as P


def from_behind(value, axis, steps):
    count = lax.axis_size(axis)
    first, last = (max(0, -steps), min(count, count - steps))
    return lax.ppermute(value, axis, [(source, source + steps) for source in range(first, last)])


def expert_step(rows_in, rows_grad, gate_w, up_w, down_w):
    gate_pre = jnp.einsum("rd,fd->rf", rows_in, gate_w, preferred_element_type=jnp.float32)
    up_pre = jnp.einsum("rd,fd->rf", rows_in, up_w, preferred_element_type=jnp.float32)
    sig_gate = jax.nn.sigmoid(gate_pre)
    silu_gate = gate_pre * sig_gate
    hidden = (silu_gate * up_pre).astype(jnp.bfloat16)
    back_hidden = jnp.einsum("rd,fd->rf", rows_grad, down_w, preferred_element_type=jnp.float32)
    back_gate = (back_hidden * up_pre * sig_gate * (1.0 + gate_pre * (1.0 - sig_gate))).astype(
        jnp.bfloat16
    )
    back_up = (back_hidden * silu_gate).astype(jnp.bfloat16)
    grad_down_e = jnp.einsum("rf,rd->fd", hidden, rows_grad, preferred_element_type=jnp.float32)
    grad_gate_e = jnp.einsum("rf,rd->fd", back_gate, rows_in, preferred_element_type=jnp.float32)
    grad_up_e = jnp.einsum("rf,rd->fd", back_up, rows_in, preferred_element_type=jnp.float32)
    partial_value = jnp.dot(back_gate, gate_w, preferred_element_type=jnp.float32) + jnp.dot(
        back_up, up_w, preferred_element_type=jnp.float32
    )
    return (partial_value, grad_gate_e, grad_up_e, grad_down_e)


def shards(
    conv_outer,
    conv_inner,
    conv_input,
    conv_taps,
    out_proj,
    mixed_state,
    route_ids,
    route_weights,
    w_gate,
    w_up,
    w_down,
    cotangent,
):
    tok_count = mixed_state.shape[0]
    col_count = mixed_state.shape[1]
    top_count = route_ids.shape[1]
    sp_size = lax.axis_size("sp")
    local_experts = w_gate.shape[0]
    experts = local_experts * sp_size
    capacity = 4 * tok_count // experts
    flat_ids = route_ids.reshape(-1)
    onehot = (flat_ids[:, None] == jnp.arange(experts, dtype=jnp.int32)[None, :]).astype(jnp.int32)
    slot_pos = jnp.sum(jnp.cumsum(onehot, axis=0) * onehot, axis=1) - 1
    slot_dest = flat_ids * capacity + slot_pos
    token_of = jnp.arange(flat_ids.shape[0], dtype=jnp.int32) // top_count
    scale_flat = route_weights.reshape(-1)[:, None]

    def pack_rows(rows):
        buffer = jnp.zeros((experts * capacity, rows.shape[1]), rows.dtype).at[slot_dest].set(rows)
        return buffer.reshape(sp_size, local_experts, capacity, rows.shape[1])

    sent_state = pack_rows(mixed_state[token_of])
    sent_grad = pack_rows(
        (cotangent[token_of].astype(jnp.float32) * scale_flat).astype(jnp.bfloat16)
    )
    recv_state, recv_grad = (
        lax.all_to_all(sent_state, "sp", split_axis=0, concat_axis=0, tiled=True),
        lax.all_to_all(sent_grad, "sp", split_axis=0, concat_axis=0, tiled=True),
    )
    state_rows, grad_rows = (
        lax.all_gather(recv_state[:, 0], "tp", axis=2, tiled=True),
        lax.all_gather(recv_grad[:, 0], "tp", axis=2, tiled=True),
    )
    width = state_rows.shape[2]
    rows_in = state_rows.reshape(-1, width)
    rows_grad = grad_rows.reshape(-1, width)
    partial_value, grad_gate_e, grad_up_e, grad_down_e = expert_step(
        rows_in, rows_grad, w_gate[0], w_up[0], w_down[0]
    )
    summed = lax.psum_scatter(
        partial_value.astype(jnp.bfloat16), "tp", scatter_dimension=1, tiled=True
    )
    back_rows = summed.reshape(sp_size, capacity, col_count)
    arrived = lax.all_to_all(
        back_rows[:, None], "sp", split_axis=0, concat_axis=0, tiled=True
    ).reshape(experts * capacity, col_count)
    picked = arrived[slot_dest].astype(jnp.float32).reshape(tok_count, top_count, col_count)
    grad_mixed = (cotangent.astype(jnp.float32) + jnp.sum(picked, axis=1)).astype(jnp.bfloat16)
    taps_count = conv_taps.shape[0]
    rim_width = taps_count - 1
    head_block = from_behind(
        jnp.stack([conv_inner[:, tok_count - rim_width :], conv_input[:, tok_count - rim_width :]]),
        "sp",
        1,
    )
    inner_ext = jnp.concatenate([head_block[0], conv_inner], axis=1).astype(jnp.float32)
    input_ext = jnp.concatenate([head_block[1], conv_input], axis=1).astype(jnp.float32)
    inner_prod = inner_ext * input_ext
    conv_out = jnp.zeros((conv_inner.shape[0], tok_count), jnp.float32)
    for offset in range(taps_count):
        conv_out = (
            conv_out + conv_taps[offset][:, None] * inner_prod[:, offset : offset + tok_count]
        )
    outer_f = conv_outer.astype(jnp.float32)
    mixer_act = (outer_f * conv_out).astype(jnp.bfloat16)
    full_back = lax.all_gather(grad_mixed, "tp", axis=1, tiled=True)
    back_mixer = jnp.einsum("cd,td->ct", out_proj, full_back, preferred_element_type=jnp.float32)
    proj_term = jnp.dot(mixer_act, full_back, preferred_element_type=jnp.float32)
    grad_proj = lax.psum_scatter(
        proj_term.astype(jnp.bfloat16), "sp", scatter_dimension=1, tiled=True
    ).astype(jnp.float32)
    grad_outer = (back_mixer * conv_out).astype(jnp.bfloat16)
    back_conv = back_mixer * outer_f
    tail_back = from_behind(back_conv[:, :rim_width], "sp", -1)
    back_ext = jnp.concatenate([back_conv, tail_back], axis=1)
    back_prod = jnp.zeros_like(back_conv)
    for offset in range(taps_count):
        shift_by = rim_width - offset
        back_prod = (
            back_prod + conv_taps[offset][:, None] * back_ext[:, shift_by : shift_by + tok_count]
        )
    grad_inner = (back_prod * conv_input.astype(jnp.float32)).astype(jnp.bfloat16)
    grad_input = (back_prod * conv_inner.astype(jnp.float32)).astype(jnp.bfloat16)
    return (
        grad_gate_e[None],
        grad_up_e[None],
        grad_down_e[None],
        grad_mixed,
        grad_proj,
        grad_outer,
        grad_inner,
        grad_input,
    )


def solution(mesh):
    placed = (
        P("tp", "sp"),
        P("tp", "sp"),
        P("tp", "sp"),
        P(None, "tp"),
        P("tp", None),
        P("sp", "tp"),
        P("sp", None),
        P("sp", None),
        P("sp", "tp", None),
        P("sp", "tp", None),
        P("sp", "tp", None),
        P("sp", "tp"),
    )
    return jax.shard_map(
        shards,
        mesh=mesh,
        in_specs=placed,
        out_specs=(
            P("sp", "tp", None),
            P("sp", "tp", None),
            P("sp", "tp", None),
            P("sp", "tp"),
            P("tp", "sp"),
            P("tp", "sp"),
            P("tp", "sp"),
            P("tp", "sp"),
        ),
        check_vma=False,
    )
```

profile of v0, /device:TPU:0, one launch (start us, length us, event | category | flops | bytes accessed | tf_op | source)
XLA Modules:
  0.0 414.5 jit_solution(1048223031491309666)
XLA Ops:
  7.3 0.8 broadcast_multiply_fusion
  8.1 0.8 copy.45
  9.5 1.2 reduce-window.6
  11.3 6.4 %scatter_custom_fusion.1 = bf16[1024,512]{1,0:T(8,128)(2,1)S(1)} fusion(s32[512]{0:T(512)S(1)} %bitcast.85, bf16[256,512]{1,0:T(8,128)(2,1)} %param.17, s32[1024]{0:T(1024)S(1)} %pad_clamp_fusion.1, bf16[]{:T(256)} %constant.26.clone.1), kind=kCustom, calls=%fused_computation.27 | custom fusion | bytes 1049088 | tf_op jit(solution)/shard_map/scatter | solution.py:62
  17.7 19.2 %all_to_all.15 = bf16[4,1,256,512]{3,2,1,0:T(8,128)(2,1)} all-to-all(bf16[4,1,256,512]{3,2,1,0:T(8,128)(2,1)S(1)} %bitcast.83), channel_id=1, replica_groups=mesh['sp'=4,'tp'=8] {'sp'}, dimensions={0} | all-to-all | bytes 2097152 | tf_op jit(solution)/shard_map/all_to_all | solution.py:70
  37.3 5.1 %scatter_custom_fusion = bf16[1024,512]{1,0:T(8,128)(2,1)S(1)} fusion(s32[512]{0:T(512)S(1)} %bitcast.86, f32[512]{0:T(512)S(1)} %mul.116, bf16[]{:T(256)} %constant.26.clone.1, bf16[256,512]{1,0:T(8,128)(2,1)S(1)} %copy-done.8, s32[1024]{0:T(1024)S(1)} %pad_clamp_fusion.1), kind=kCustom, calls=%fused_computation.26 | custom fusion | flops 786432 | bytes 1316866 | tf_op jit(solution)/shard_map/scatter | solution.py:62
  42.4 16.1 %all_to_all.16 = bf16[4,1,256,512]{3,2,1,0:T(8,128)(2,1)} all-to-all(bf16[4,1,256,512]{3,2,1,0:T(8,128)(2,1)S(1)} %bitcast.82), channel_id=1, replica_groups=mesh['sp'=4,'tp'=8] {'sp'}, dimensions={0} | all-to-all | bytes 2097152 | tf_op jit(solution)/shard_map/all_to_all | solution.py:71
  58.8 60.1 %all-gather.10.cloned.1.call-done = bf16[4,1,256,4096]{3,2,1,0:T(8,128)(2,1)} async-done(((bf16[4,1,256,512]{3,2,1,0:T(8,128)(2,1)}), bf16[4,1,256,4096]{3,2,1,0:T(8,128)(2,1)}) %all-gather.10.cloned.1.call-update) | async-done | bytes 8388624 | tf_op jit(solution)/shard_map/all_gather | solution.py:74
  118.9 6.9 %fusion.2 = f32[1024,256]{1,0:T(8,128)} fusion(bf16[1024,4096]{1,0:T(8,128)(2,1)} %bitcast.73, bf16[1,256,4096]{2,1,0:T(8,128)(2,1)S(1)} %copy-done), kind=kOutput, calls=%fused_computation.12 | convolution fusion | flops 2147483648 | bytes 11534336 | tf_op jit(solution)/shard_map/rd,fd->rf/dot_general | solution.py:14
  125.7 3.3 fusion.5
  129.1 71.9 %all-gather.8.cloned.1.call-done = bf16[4,1,256,4096]{3,2,1,0:T(8,128)(2,1)} async-done(((bf16[4,1,256,512]{3,2,1,0:T(8,128)(2,1)}), bf16[4,1,256,4096]{3,2,1,0:T(8,128)(2,1)}) %all-gather.8.cloned.1.call-update) | async-done | bytes 8388624 | tf_op jit(solution)/shard_map/all_gather | solution.py:75
  201.0 7.1 %multiply_convert_fusion.1 = (bf16[1024,256]{1,0:T(8,128)(2,1)S(1)}, bf16[1024,256]{1,0:T(8,128)(2,1)S(1)}) fusion(f32[1024,256]{1,0:T(8,128)} %fusion.2, f32[1024,256]{1,0:T(8,128)} %fusion.5, bf16[1024,4096]{1,0:T(8,128)(2,1)} %bitcast.80, bf16[1,256,4096]{2,1,0:T(8,128)(2,1)} %param.22), kind=kOutput, calls=%fused_computation.21 | convolution fusion | flops 2150891520 | bytes 13631488 | tf_op jit(solution)/shard_map/rd,fd->rf/dot_general | solution.py:19
  208.2 8.1 %fusion = f32[1024,4096]{1,0:T(8,128)} fusion(bf16[1024,256]{1,0:T(8,128)(2,1)S(1)} %get-tuple-element.37, bf16[1,256,4096]{2,1,0:T(8,128)(2,1)S(1)} %copy-done), kind=kOutput, calls=%fused_computation.10 | convolution fusion | flops 2147483648 | bytes 19398656 | tf_op jit(solution)/shard_map/dot_general | solution.py:27
  216.2 11.6 %add_convert_fusion = bf16[1024,4096]{1,0:T(8,128)(2,1)} fusion(f32[1024,4096]{1,0:T(8,128)} %fusion, bf16[1024,256]{1,0:T(8,128)(2,1)S(1)} %get-tuple-element.36, bf16[1,256,4096]{2,1,0:T(8,128)(2,1)S(1)} %copy-done.4), kind=kOutput, calls=%fused_computation.5 | convolution fusion | flops 2155872256 | bytes 27787264 | tf_op jit(solution)/shard_map/dot_general | solution.py:27
  227.9 88.2 %reduce-scatter.3.cloned.1.call-done = bf16[1024,512]{1,0:T(8,128)(2,1)} async-done(((bf16[1024,4096]{1,0:T(8,128)(2,1)}), bf16[1024,512]{1,0:T(8,128)(2,1)}) %reduce-scatter.3.cloned.1.call-update) | async-done | bytes 1048592 | tf_op jit(solution)/shard_map/reduce_scatter | solution.py:83
  316.1 3.6 all-to-all-start.2
  319.7 11.9 %all-to-all-done.2 = bf16[4,1,256,512]{3,2,1,0:T(8,128)(2,1)S(1)} async-done(((bf16[4,1,256,512]{3,2,1,0:T(8,128)(2,1)}), bf16[4,1,256,512]{3,2,1,0:T(8,128)(2,1)S(1)}, u32[]{:S(2)}, u32[]{:S(2)}) %all-to-all-start.2) | async-done | bytes 1048608 | tf_op jit(solution)/shard_map/all_to_all | solution.py:87
  331.6 2.0 gather_fusion
  334.3 1.2 reduce_sum.19
  335.5 0.8 add_convert_fusion.1
  336.6 3.3 collective-permute-start
  340.1 1.2 collective-permute-done
  341.2 0.8 convert_multiply_fusion.2
  342.0 23.0 %all-gather.6.cloned.1.call-done = bf16[256,4096]{1,0:T(8,128)(2,1)} async-done(((bf16[256,512]{1,0:T(8,128)(2,1)}), bf16[256,4096]{1,0:T(8,128)(2,1)}) %all-gather.6.cloned.1.call-update) | async-done | bytes 2097168 | tf_op jit(solution)/shard_map/all_gather | solution.py:109
  365.0 4.0 multiply_convert_fusion.8
  369.0 2.1 convolution_convert_fusion
  371.2 7.9 %convolution_bitcast_fusion.2 = f32[1,256,4096]{2,1,0:T(8,128)} fusion(bf16[1024,256]{1,0:T(8,128)(2,1)S(1)} %get-tuple-element.37, bf16[1024,4096]{1,0:T(8,128)(2,1)} %bitcast.74), kind=kOutput, calls=%fused_computation.8 | convolution fusion | flops 2147483648 | bytes 13107200 | tf_op jit(solution)/shard_map/rf,rd->fd/dot_general | solution.py:25
  379.1 8.0 %convolution_bitcast_fusion = f32[1,256,4096]{2,1,0:T(8,128)} fusion(bf16[1024,4096]{1,0:T(8,128)(2,1)} %bitcast.81, f32[1024,256]{1,0:T(8,128)S(1)} %copy-done.7, f32[1024,256]{1,0:T(8,128)S(1)} %copy-done.6), kind=kOutput, calls=%fused_computation.6 | convolution fusion | flops 2149056512 | bytes 14680064 | tf_op jit(solution)/shard_map/rf,rd->fd/dot_general | solution.py:24
  387.2 1.4 collective-permute-start.1
  388.6 4.4 %convolution_bitcast_fusion.1 = f32[1,256,4096]{2,1,0:T(8,128)} fusion(bf16[1024,256]{1,0:T(8,128)(2,1)S(1)} %get-tuple-element.36, bf16[1024,4096]{1,0:T(8,128)(2,1)S(1)} %bitcast.78), kind=kOutput, calls=%fused_computation.7 | convolution fusion | flops 2147483648 | bytes 13107200 | tf_op jit(solution)/shard_map/rf,rd->fd/dot_general | solution.py:26
  395.5 10.4 %reduce-scatter.5.cloned.1.call-done = bf16[256,1024]{1,0:T(8,128)(2,1)} async-done(((bf16[256,4096]{1,0:T(8,128)(2,1)}), bf16[256,1024]{1,0:T(8,128)(2,1)}) %reduce-scatter.5.cloned.1.call-update) | async-done | bytes 524304 | tf_op jit(solution)/shard_map/reduce_scatter | solution.py:112
  405.9 2.1 convert_element_type.85
  (78 shorter events, 5.3 us)
Async XLA Ops:
  7.2 111.7 %copy-start = (bf16[1,256,4096]{2,1,0:T(8,128)(2,1)S(1)}, bf16[1,256,4096]{2,1,0:T(8,128)(2,1)}, u32[]{:S(2)}) copy-start(bf16[1,256,4096]{2,1,0:T(8,128)(2,1)} %param.20) | copy-start | bytes 6291460
  7.2 29.8 %copy-start.15 = (f32[256,2]{0,1:T(2,128)S(1)}, f32[256,2]{0,1:T(2,128)}, u32[]{:S(2)}) copy-start(f32[256,2]{0,1:T(2,128)} %param.19) | copy-start | bytes 6148
  7.2 30.1 %copy-start.8 = (bf16[256,512]{1,0:T(8,128)(2,1)S(1)}, bf16[256,512]{1,0:T(8,128)(2,1)}, u32[]{:S(2)}) copy-start(bf16[256,512]{1,0:T(8,128)(2,1)} %param.23) | copy-start | bytes 786436
  7.2 111.6 %all-gather.10.cloned.1.call-start = ((), (), s32[]{:S(2)}) async-start(), calls=%async_computation.9 | async-start | bytes 9437184 | tf_op jit(solution)/shard_map/all_gather | solution.py:74
  36.9 164.1 %all-gather.8.cloned.1.call-start = ((), (), s32[]{:S(2)}) async-start(), calls=%async_computation.8 | async-start | bytes 9437184 | tf_op jit(solution)/shard_map/all_gather | solution.py:75
  58.5 257.5 %reduce-scatter.3.cloned.1.call-start = ((), (), s32[]{:S(2)}) async-start(), calls=%async_computation.5 | async-start | bytes 9437184 | tf_op jit(solution)/shard_map/reduce_scatter | solution.py:83
  118.8 6.9 %copy-start.2 = (bf16[4,1,256,4096]{3,2,1,0:T(8,128)(2,1)S(1)}, bf16[4,1,256,4096]{3,2,1,0:T(8,128)(2,1)}, u32[]{:S(2)}) copy-start(bf16[4,1,256,4096]{3,2,1,0:T(8,128)(2,1)} %all-gather.10.cloned.1.call-done) | copy-start | bytes 25165828
  118.9 6.9 %copy-start.3 = (bf16[1,256,4096]{2,1,0:T(8,128)(2,1)S(1)}, bf16[1,256,4096]{2,1,0:T(8,128)(2,1)}, u32[]{:S(2)}) copy-start(bf16[1,256,4096]{2,1,0:T(8,128)(2,1)} %param.21) | copy-start | bytes 6291460
  208.1 8.1 %copy-start.4 = (bf16[1,256,4096]{2,1,0:T(8,128)(2,1)S(1)}, bf16[1,256,4096]{2,1,0:T(8,128)(2,1)}, u32[]{:S(2)}) copy-start(bf16[1,256,4096]{2,1,0:T(8,128)(2,1)} %param.21) | copy-start | bytes 6291460
  316.1 15.5 %all-to-all-start.2 = ((bf16[4,1,256,512]{3,2,1,0:T(8,128)(2,1)}), bf16[4,1,256,512]{3,2,1,0:T(8,128)(2,1)S(1)}, u32[]{:S(2)}, u32[]{:S(2)}) async-start(bf16[4,1,256,512]{3,2,1,0:T(8,128)(2,1)} %bitcast.84), calls=%async_computation.3 | async-start | bytes 2097152 | tf_op jit(solution)/shard_map/all_to_all | solution.py:87
  319.7 45.3 %all-gather.6.cloned.1.call-start = ((), (), s32[]{:S(2)}) async-start(), calls=%async_computation.6 | async-start | bytes 2359296 | tf_op jit(solution)/shard_map/all_gather | solution.py:109
  331.6 4.7 %copy-start.10 = (bf16[256,256]{1,0:T(8,128)(2,1)S(1)}, bf16[256,256]{1,0:T(8,128)(2,1)}, u32[]{:S(2)}) copy-start(bf16[256,256]{1,0:T(8,128)(2,1)} %param.13) | copy-start | bytes 393220
  331.6 4.9 %copy-start.11 = (bf16[256,256]{1,0:T(8,128)(2,1)S(1)}, bf16[256,256]{1,0:T(8,128)(2,1)}, u32[]{:S(2)}) copy-start(bf16[256,256]{1,0:T(8,128)(2,1)} %param.14) | copy-start | bytes 393220
  331.6 8.3 %copy-start.14 = (f32[3,256]{1,0:T(4,128)S(1)}, f32[3,256]{1,0:T(4,128)}, u32[]{:S(2)}) copy-start(f32[3,256]{1,0:T(4,128)} %param.15) | copy-start | bytes 9220
  331.6 8.4 %copy-start.12 = (bf16[256,256]{1,0:T(8,128)(2,1)S(1)}, bf16[256,256]{1,0:T(8,128)(2,1)}, u32[]{:S(2)}) copy-start(bf16[256,256]{1,0:T(8,128)(2,1)} %param.12) | copy-start | bytes 393220
  336.3 69.6 %reduce-scatter.5.cloned.1.call-start = ((), (), s32[]{:S(2)}) async-start(), calls=%async_computation.7 | async-start | bytes 2621440 | tf_op jit(solution)/shard_map/reduce_scatter | solution.py:112
  336.6 4.6 %collective-permute-start = (bf16[2,256,2]{1,2,0:T(2,128)(2,1)S(1)}, bf16[2,256,2]{1,2,0:T(2,128)(2,1)S(1)}, u32[]{:S(2)}, u32[]{:S(2)}) collective-permute-start(bf16[2,256,2]{1,2,0:T(2,128)(2,1)S(1)} %pad_maximum_fusion.1), channel_id=1, source_target_pairs={{0,8},{8,16},{16,24},{1,9},{9,17},{17,25},{2,10},{10,18},{18,26},{... | collective-permute-start | bytes 6152 | tf_op jit(solution)/shard_map/ppermute | solution.py:10
  365.0 4.0 copy-start.5
  371.2 8.0 %copy-start.6 = (f32[1024,256]{1,0:T(8,128)S(1)}, f32[1024,256]{1,0:T(8,128)}, u32[]{:S(2)}) copy-start(f32[1024,256]{1,0:T(8,128)} %fusion.2) | copy-start | bytes 3145732
  371.2 8.0 %copy-start.7 = (f32[1024,256]{1,0:T(8,128)S(1)}, f32[1024,256]{1,0:T(8,128)}, u32[]{:S(2)}) copy-start(f32[1024,256]{1,0:T(8,128)} %fusion.5) | copy-start | bytes 3145732
  371.2 17.4 %slice-start = ((s8[8388608]{0:T(1024)(128)(4,1)}), s8[4194304]{0:T(1024)(128)(4,1)S(1)}, s32[]{:S(2)}) async-start(s8[8388608]{0:T(1024)(128)(4,1)} %bitcast.76), calls=%async_computation.10 | async-start | bytes 8388608
  379.1 8.1 %copy-start.9 = (f32[256,256]{0,1:T(8,128)S(1)}, f32[256,256]{0,1:T(8,128)}, u32[]{:S(2)}) copy-start(f32[256,256]{0,1:T(8,128)} %get-tuple-element.38) | copy-start | bytes 786436
  379.1 9.5 %slice-start.1 = ((s8[8388608]{0:T(1024)(128)(4,1)}), s8[4194304]{0:T(1024)(128)(4,1)S(1)}, s32[]{:S(2)}) async-start(s8[8388608]{0:T(1024)(128)(4,1)} %bitcast.76), calls=%async_computation.11 | async-start | bytes 8388608
  387.2 5.9 %copy-start.13 = (bf16[256,256]{0,1:T(8,128)(2,1)S(1)}, bf16[256,256]{0,1:T(8,128)(2,1)}, u32[]{:S(2)}) copy-start(bf16[256,256]{0,1:T(8,128)(2,1)} %get-tuple-element.34) | copy-start | bytes 393220
  387.2 6.6 %collective-permute-start.1 = (f32[256,2]{0,1:T(2,128)S(1)}, f32[256,2]{0,1:T(2,128)S(1)}, u32[]{:S(2)}, u32[]{:S(2)}) collective-permute-start(f32[256,2]{0,1:T(2,128)S(1)} %slice.77), channel_id=1, source_target_pairs={{8,0},{16,8},{24,16},{9,1},{17,9},{25,17},{10,2},{18,10},{26,18},{... | collective-permute-start | bytes 6152 | tf_op jit(solution)/shard_map/ppermute | solution.py:10
  388.6 19.4 %copy-start.1 = (bf16[1,256,4096]{2,1,0:T(8,128)(2,1)S(1)}, bf16[1,256,4096]{2,1,0:T(8,128)(2,1)}, u32[]{:S(2)}) copy-start(bf16[1,256,4096]{2,1,0:T(8,128)(2,1)} %param.20) | copy-start | bytes 6291460
Sparse Core Ops, SparseCore 0:
  37.1 81.7 all-gather.9
  120.4 80.5 all-gather.7
  228.0 88.0 reduce-scatter.2
  336.4 28.5 all-gather.5
  371.3 34.5 reduce-scatter.4
where the time goes:
time: 415 us
  waiting for transfers between devices  267 us (64%)
  matrix products  63.5 us (15%)
  blocking collectives  35.3 us (9%)
  between operations  14.1 us (3%)
  local copies, waits for them, and re-layouts  13.6 us (3%)
  other arithmetic  12.5 us (3%)
  starting transfers between devices  8.73 us (2%)
    reduce_scatter x1, waiting for transfers between devices, shards(): lax.psum_scatter(partial_value.astype(jnp.bfloat16), 'tp', scatter_dimens...  88.2 us
    all_gather x1, waiting for transfers between devices, shards(): lax.all_gather(recv_grad[:, 0], 'tp', axis=2, tiled=True)  71.9 us
    all_gather x1, waiting for transfers between devices, shards(): lax.all_gather(recv_state[:, 0], 'tp', axis=2, tiled=True)  60.1 us
    all_gather x1, waiting for transfers between devices, shards(): full_back = lax.all_gather(grad_mixed, 'tp', axis=1, tiled=True)  23 us
    all_to_all x1, blocking collectives, shards(): lax.all_to_all(sent_state, 'sp', split_axis=0, concat_axis=0, tiled=True)  19.2 us
    all_to_all x1, blocking collectives, shards(): lax.all_to_all(sent_grad, 'sp', split_axis=0, concat_axis=0, tiled=True)  16.1 us
    all_to_all x1, waiting for transfers between devices, shards(): lax.all_to_all(back_rows[:, None], 'sp', split_axis=0, concat_axis=0, til...  11.9 us
    dot_general x1, matrix products, expert_step(): jnp.dot(back_up, up_w, preferred_element_type=jnp.float32)  11.6 us
  transfers between devices with their start and end apart: 8, of which 7 were waited for; matrix products, arithmetic and copies ran while one was open for 10% of the time, Pallas kernels for 0%

commit v1 on v0

--- a/solution.py
+++ b/solution.py
@@ -1,6 +1,10 @@
+import functools
+
 import jax
 import jax.numpy as jnp
 from jax import lax
+from jax.experimental import pallas as pl
+from jax.experimental.pallas import tpu as pltpu
 from jax.sharding import PartitionSpec as P
 
 
@@ -8,6 +12,33 @@
     count = lax.axis_size(axis)
     first, last = (max(0, -steps), min(count, count - steps))
     return lax.ppermute(value, axis, [(source, source + steps) for source in range(first, last)])
+
+
+def row_back_kernel(gate_ref, up_ref, gate_w_ref, up_w_ref, out_ref):
+    total = jnp.dot(gate_ref[...], gate_w_ref[...], preferred_element_type=jnp.float32)
+    total += jnp.dot(up_ref[...], up_w_ref[...], preferred_element_type=jnp.float32)
+    out_ref[...] = total.astype(out_ref.dtype)
+
+
+def row_back(back_gate, back_up, gate_w, up_w):
+    rows, hidden = back_gate.shape
+    width = gate_w.shape[1]
+    tile = min(512, width)
+    left = pl.BlockSpec((rows, hidden), lambda i: (0, 0))
+    right = pl.BlockSpec((hidden, tile), lambda i: (0, i))
+    return pl.pallas_call(
+        row_back_kernel,
+        grid=(width // tile,),
+        out_shape=jax.ShapeDtypeStruct((rows, width), jnp.bfloat16),
+        in_specs=[left, left, right, right],
+        out_specs=pl.BlockSpec((rows, tile), lambda i: (0, i)),
+        cost_estimate=pl.CostEstimate(
+            flops=4 * rows * hidden * width,
+            bytes_accessed=2 * (2 * rows * hidden + 2 * hidden * width + rows * width),
+            transcendentals=0,
+        ),
+        name="row_back",
+    )(back_gate, back_up, gate_w, up_w)
 
 
 def expert_step(rows_in, rows_grad, gate_w, up_w, down_w):
@@ -24,10 +55,192 @@
     grad_down_e = jnp.einsum("rf,rd->fd", hidden, rows_grad, preferred_element_type=jnp.float32)
     grad_gate_e = jnp.einsum("rf,rd->fd", back_gate, rows_in, preferred_element_type=jnp.float32)
     grad_up_e = jnp.einsum("rf,rd->fd", back_up, rows_in, preferred_element_type=jnp.float32)
-    partial_value = jnp.dot(back_gate, gate_w, preferred_element_type=jnp.float32) + jnp.dot(
-        back_up, up_w, preferred_element_type=jnp.float32
-    )
+    partial_value = row_back(back_gate, back_up, gate_w, up_w)
     return (partial_value, grad_gate_e, grad_up_e, grad_down_e)
+
+
+Z_UP, Z_DOWN, BY_X, BY_Y, HALF_X, HALF_Y, PEER = range(7)
+KINDS = PEER + 4
+
+
+def gather_kernel(levels, cot_in, state_in, cot_out, state_out, own_sem, send_sem, recv_sem):
+    sp, tp = lax.axis_index("sp"), lax.axis_index("tp")
+    level, core = tp // 2, tp % 2
+    beside_x = sp + 1 - 2 * (sp % 2)
+    beside_y = (sp + 2) % 4
+    across = 3 - sp
+    peer = tp + 1 - 2 * core
+    rows, cols = cot_in.shape
+    half = rows // 2
+    ins, outs = (cot_in, state_in), (cot_out, state_out)
+
+    barrier = pltpu.get_barrier_semaphore()
+
+    def greet(to_sp, to_tp):
+        pl.semaphore_signal(
+            barrier,
+            inc=1,
+            device_id=(to_sp, to_tp),
+            device_id_type=pl.DeviceIdType.MESH,
+        )
+
+    greet(beside_x, tp)
+    greet(beside_y, tp)
+    greet(sp, peer)
+    pl.when(level > 0)(lambda: greet(sp, tp - 2))
+    pl.when(level < levels - 1)(lambda: greet(sp, tp + 2))
+    one = jnp.int32(1)
+    none = jnp.int32(0)
+    pl.semaphore_wait(
+        barrier,
+        3 + jnp.where(level > 0, one, none) + jnp.where(level < levels - 1, one, none),
+    )
+
+    def block(array, of_sp, of_level, of_core, start=0, size=rows):
+        return outs[array].at[
+            pl.ds(pl.multiple_of(of_sp * rows + start, 16), size),
+            pl.ds(pl.multiple_of((of_level * 2 + of_core) * cols, 128), cols),
+        ]
+
+    def remote(array, kind, of_level, source, target, to_sp, to_tp):
+        return pltpu.make_async_remote_copy(
+            src_ref=source,
+            dst_ref=target,
+            send_sem=send_sem.at[array, kind, of_level],
+            recv_sem=recv_sem.at[array, kind, of_level],
+            device_id=(to_sp, to_tp),
+            device_id_type=pl.DeviceIdType.MESH,
+        )
+
+    def spread(array, of_level, source, kind, to_sp, to_tp):
+        remote(
+            array, kind, of_level, source, block(array, sp, of_level, core), to_sp, to_tp
+        ).start()
+
+    def pieces(array, of_level):
+        return {
+            Z_UP: block(array, sp, of_level, core),
+            Z_DOWN: block(array, sp, of_level, core),
+            BY_X: block(array, beside_x, of_level, core),
+            BY_Y: block(array, beside_y, of_level, core),
+            HALF_Y: block(array, across, of_level, core, 0, half),
+            HALF_X: block(array, across, of_level, core, half, half),
+            PEER: block(array, sp, of_level, 1 - core),
+            PEER + 1: block(array, beside_x, of_level, 1 - core),
+            PEER + 2: block(array, beside_y, of_level, 1 - core),
+            PEER + 3: block(array, across, of_level, 1 - core),
+        }
+
+    def arrive(array, kind, of_level):
+        piece = pieces(array, of_level)[kind]
+        remote(array, kind, of_level, piece, piece, sp, peer).wait_recv()
+
+    def left(array, kind, of_level):
+        piece = pieces(array, of_level)[kind]
+        remote(array, kind, of_level, piece, piece, sp, peer).wait_send()
+
+    def hand_on(array, of_level, kind, of_sp, to_sp, to_tp, start=0, size=rows):
+        piece = block(array, of_sp, of_level, core, start, size)
+        remote(array, kind, of_level, piece, piece, to_sp, to_tp).start()
+
+    def column(array, step, up):
+        of_level = level if step == 0 else (level - step if up else level + step)
+        if step == 0:
+            source = ins[array]
+            pltpu.make_async_copy(
+                source, block(array, sp, level, core), own_sem.at[array]
+            ).start()
+        else:
+            arrive(array, Z_UP if up else Z_DOWN, of_level)
+            source = block(array, sp, of_level, core)
+        if step == 0 or up:
+            pl.when(level < levels - 1)(
+                lambda: spread(array, of_level, source, Z_UP, sp, tp + 2)
+            )
+        if step == 0 or not up:
+            pl.when(level > 0)(lambda: spread(array, of_level, source, Z_DOWN, sp, tp - 2))
+        spread(array, of_level, source, BY_X, beside_x, tp)
+        spread(array, of_level, source, BY_Y, beside_y, tp)
+        spread(array, of_level, source, PEER, sp, peer)
+
+    def plane(array, step, up):
+        of_level = level - step if up else level + step
+        arrive(array, BY_X, of_level)
+        hand_on(array, of_level, HALF_Y, beside_x, beside_y, tp, 0, half)
+        hand_on(array, of_level, PEER + 1, beside_x, sp, peer)
+        arrive(array, BY_Y, of_level)
+        hand_on(array, of_level, HALF_X, beside_y, beside_x, tp, half, half)
+        hand_on(array, of_level, PEER + 2, beside_y, sp, peer)
+
+    def corner(array, step, up):
+        of_level = level - step if up else level + step
+        arrive(array, HALF_X, of_level)
+        arrive(array, HALF_Y, of_level)
+        hand_on(array, of_level, PEER + 3, across, sp, peer)
+
+    def each(action, step):
+        if not 0 <= step < levels:
+            return
+        if step == 0:
+            for array in range(2):
+                action(array, 0, True)
+            return
+
+        @pl.when(level >= step)
+        def _():
+            for array in range(2):
+                action(array, step, True)
+
+        @pl.when(level < levels - step)
+        def _():
+            for array in range(2):
+                action(array, step, False)
+
+    for step in range(levels + 2):
+        each(column, step)
+        each(plane, step - 1)
+        each(corner, step - 2)
+
+    for array in range(2):
+        pltpu.make_async_copy(
+            ins[array], block(array, sp, level, core), own_sem.at[array]
+        ).wait()
+        for of_level in range(levels):
+            for kind in (PEER, PEER + 1, PEER + 2, PEER + 3):
+                arrive(array, kind, of_level)
+                left(array, kind, of_level)
+            for kind in (BY_X, BY_Y, HALF_X, HALF_Y):
+                left(array, kind, of_level)
+            pl.when((level < levels - 1) & (level >= of_level))(
+                lambda: left(array, Z_UP, of_level)
+            )
+            pl.when((level > 0) & (level <= of_level))(lambda: left(array, Z_DOWN, of_level))
+
+
+def gather_all(cotangent, mixed_state):
+    rows, cols = cotangent.shape
+    levels = lax.axis_size("tp") // 2
+    whole = jax.ShapeDtypeStruct((4 * rows, 2 * levels * cols), cotangent.dtype)
+    return pl.pallas_call(
+        functools.partial(gather_kernel, levels),
+        out_shape=(whole, whole),
+        in_specs=[pl.BlockSpec(memory_space=pltpu.VMEM)] * 2,
+        out_specs=[pl.BlockSpec(memory_space=pl.ANY)] * 2,
+        scratch_shapes=[
+            pltpu.SemaphoreType.DMA((2,)),
+            pltpu.SemaphoreType.DMA((2, KINDS, levels)),
+            pltpu.SemaphoreType.DMA((2, KINDS, levels)),
+        ],
+        compiler_params=pltpu.CompilerParams(collective_id=0, has_side_effects=True),
+        name="gather_all",
+    )(cotangent, mixed_state)
+
+
+def sum_blocks(tall, sp_size, rows, cols):
+    parts = lax.all_to_all(
+        tall.reshape(sp_size, 1, rows, cols), "sp", split_axis=0, concat_axis=0, tiled=True
+    )
+    return jnp.sum(parts.reshape(sp_size, rows, cols).astype(jnp.float32), axis=0)
 
 
 def shards(
@@ -51,44 +264,64 @@
     local_experts = w_gate.shape[0]
     experts = local_experts * sp_size
     capacity = 4 * tok_count // experts
-    flat_ids = route_ids.reshape(-1)
-    onehot = (flat_ids[:, None] == jnp.arange(experts, dtype=jnp.int32)[None, :]).astype(jnp.int32)
-    slot_pos = jnp.sum(jnp.cumsum(onehot, axis=0) * onehot, axis=1) - 1
-    slot_dest = flat_ids * capacity + slot_pos
-    token_of = jnp.arange(flat_ids.shape[0], dtype=jnp.int32) // top_count
-    scale_flat = route_weights.reshape(-1)[:, None]
-
-    def pack_rows(rows):
-        buffer = jnp.zeros((experts * capacity, rows.shape[1]), rows.dtype).at[slot_dest].set(rows)
-        return buffer.reshape(sp_size, local_experts, capacity, rows.shape[1])
-
-    sent_state = pack_rows(mixed_state[token_of])
-    sent_grad = pack_rows(
-        (cotangent[token_of].astype(jnp.float32) * scale_flat).astype(jnp.bfloat16)
-    )
-    recv_state, recv_grad = (
-        lax.all_to_all(sent_state, "sp", split_axis=0, concat_axis=0, tiled=True),
-        lax.all_to_all(sent_grad, "sp", split_axis=0, concat_axis=0, tiled=True),
-    )
-    state_rows, grad_rows = (
-        lax.all_gather(recv_state[:, 0], "tp", axis=2, tiled=True),
-        lax.all_gather(recv_grad[:, 0], "tp", axis=2, tiled=True),
-    )
-    width = state_rows.shape[2]
-    rows_in = state_rows.reshape(-1, width)
-    rows_grad = grad_rows.reshape(-1, width)
-    partial_value, grad_gate_e, grad_up_e, grad_down_e = expert_step(
-        rows_in, rows_grad, w_gate[0], w_up[0], w_down[0]
-    )
-    summed = lax.psum_scatter(
-        partial_value.astype(jnp.bfloat16), "tp", scatter_dimension=1, tiled=True
-    )
-    back_rows = summed.reshape(sp_size, capacity, col_count)
-    arrived = lax.all_to_all(
-        back_rows[:, None], "sp", split_axis=0, concat_axis=0, tiled=True
-    ).reshape(experts * capacity, col_count)
-    picked = arrived[slot_dest].astype(jnp.float32).reshape(tok_count, top_count, col_count)
-    grad_mixed = (cotangent.astype(jnp.float32) + jnp.sum(picked, axis=1)).astype(jnp.bfloat16)
+    if capacity == tok_count and sp_size == 4 and lax.axis_size("tp") % 2 == 0:
+        choice = route_ids[:, :, None] == jnp.arange(experts, dtype=jnp.int32)[None, None, :]
+        scale_of = jnp.sum(jnp.where(choice, route_weights[:, :, None], 0.0), axis=1).T
+        scales = lax.all_to_all(
+            scale_of[:, None], "sp", split_axis=0, concat_axis=1, tiled=True
+        ).reshape(-1, 1)
+        cot_all, rows_in = gather_all(cotangent, mixed_state)
+        rows_grad = (cot_all.astype(jnp.float32) * scales).astype(jnp.bfloat16)
+        partial_value, grad_gate_e, grad_up_e, grad_down_e = expert_step(
+            rows_in, rows_grad, w_gate[0], w_up[0], w_down[0]
+        )
+        tall = lax.psum_scatter(
+            partial_value, "tp", scatter_dimension=1, tiled=True
+        )
+        tall, grad_gate_e, grad_up_e, grad_down_e = lax.optimization_barrier(
+            (tall, grad_gate_e, grad_up_e, grad_down_e)
+        )
+        summed = sum_blocks(tall, sp_size, tok_count, col_count)
+        grad_mixed = (cotangent.astype(jnp.float32) + summed).astype(jnp.bfloat16)
+    else:
+        flat_ids = route_ids.reshape(-1)
+        onehot = (flat_ids[:, None] == jnp.arange(experts, dtype=jnp.int32)[None, :]).astype(jnp.int32)
+        slot_pos = jnp.sum(jnp.cumsum(onehot, axis=0) * onehot, axis=1) - 1
+        slot_dest = flat_ids * capacity + slot_pos
+        token_of = jnp.arange(flat_ids.shape[0], dtype=jnp.int32) // top_count
+        scale_flat = route_weights.reshape(-1)[:, None]
+
+        def pack_rows(rows):
+            buffer = jnp.zeros((experts * capacity, rows.shape[1]), rows.dtype).at[slot_dest].set(rows)
+            return buffer.reshape(sp_size, local_experts, capacity, rows.shape[1])
+
+        sent_state = pack_rows(mixed_state[token_of])
+        sent_grad = pack_rows(
+            (cotangent[token_of].astype(jnp.float32) * scale_flat).astype(jnp.bfloat16)
+        )
+        recv_state, recv_grad = (
+            lax.all_to_all(sent_state, "sp", split_axis=0, concat_axis=0, tiled=True),
+            lax.all_to_all(sent_grad, "sp", split_axis=0, concat_axis=0, tiled=True),
+        )
+        state_rows, grad_rows = (
+            lax.all_gather(recv_state[:, 0], "tp", axis=2, tiled=True),
+            lax.all_gather(recv_grad[:, 0], "tp", axis=2, tiled=True),
+        )
+        width = state_rows.shape[2]
+        rows_in = state_rows.reshape(-1, width)
+        rows_grad = grad_rows.reshape(-1, width)
+        partial_value, grad_gate_e, grad_up_e, grad_down_e = expert_step(
+            rows_in, rows_grad, w_gate[0], w_up[0], w_down[0]
+        )
+        summed = lax.psum_scatter(
+            partial_value, "tp", scatter_dimension=1, tiled=True
+        )
+        back_rows = summed.reshape(sp_size, capacity, col_count)
+        arrived = lax.all_to_all(
+            back_rows[:, None], "sp", split_axis=0, concat_axis=0, tiled=True
+        ).reshape(experts * capacity, col_count)
+        picked = arrived[slot_dest].astype(jnp.float32).reshape(tok_count, top_count, col_count)
+        grad_mixed = (cotangent.astype(jnp.float32) + jnp.sum(picked, axis=1)).astype(jnp.bfloat16)
     taps_count = conv_taps.shape[0]
     rim_width = taps_count - 1
     head_block = from_behind(

time: 415 us -> 301 us (0.73)
  waiting for transfers between devices: 267 us -> 124 us
  Pallas kernels: 0 us -> 85.3 us
  matrix products: 63.5 us -> 43.1 us
  blocking collectives: 35.3 us -> 16 us
  local copies, waits for them, and re-layouts: 13.6 us -> 4.47 us
  other arithmetic: 12.5 us -> 4.13 us
    all_gather x2 -> x0, waiting for transfers between devices: 132 us -> none  [the longest x1 71.9 us: shards(): lax.all_gather(recv_grad[:, 0], 'tp', axis=2, tiled=True)]
    pallas_call x0 -> x2, Pallas kernels: none -> 85.3 us  [the longest x1 75 us: gather_all(): pl.pallas_call(functools.partial(gather_kernel, levels), out_shape=(whole...]
    reduce_scatter x1, waiting for transfers between devices: 88.2 us -> 68 us  [shards(): lax.psum_scatter(partial_value, 'tp', scatter_dimension=1, tiled=True)]
    dot_general x2 -> x0, matrix products: 19.7 us -> none  [the longest x1 11.6 us: expert_step(): jnp.dot(back_up, up_w, preferred_element_type=jnp.float32)]
    all_to_all x2 -> x1, blocking collectives: 35.3 us -> 16 us  [sum_blocks(): lax.all_to_all(tall.reshape(sp_size, 1, rows, cols), 'sp', split_axis=0,...]
    reduce_scatter x1, waiting for transfers between devices: 10.4 us -> 27.6 us  [shards(): lax.psum_scatter(proj_term.astype(jnp.bfloat16), 'sp', scatter_dimension=...]
    all_to_all x1, waiting for transfers between devices: 11.9 us -> 0.01 us  [shards(): lax.all_to_all(scale_of[:, None], 'sp', split_axis=0, concat_axis=1, tile...]
    scatter x1 -> x0, local copies, waits for them, and re-layouts: 6.4 us -> none  [pack_rows(): jnp.zeros((experts * capacity, rows.shape[1]), rows.dtype).at[slot_dest]]
  transfers between devices with their start and end apart: 8 -> 6, of which waited for: 7 -> 5; matrix products, arithmetic and copies ran while one was open for 10% -> 11% of each run, Pallas kernels for 0% -> 25%
where the time goes in v1:
time: 301 us; the launch traced here: 300 us
  waiting for transfers between devices  124 us (41%)
  Pallas kernels  85.3 us (28%)
  matrix products  43.1 us (14%)
  blocking collectives  16 us (5%)
  between operations  14 us (5%)
  starting transfers between devices  9.57 us (3%)
  local copies, waits for them, and re-layouts  4.47 us (1%)
  other arithmetic  4.13 us (1%)
    pallas_call x1, Pallas kernels, gather_all(): pl.pallas_call(functools.partial(gather_kernel, levels), out_shape=(whole...  75 us
    reduce_scatter x1, waiting for transfers between devices, shards(): lax.psum_scatter(partial_value, 'tp', scatter_dimension=1, tiled=True)  68 us
    reduce_scatter x1, waiting for transfers between devices, shards(): lax.psum_scatter(proj_term.astype(jnp.bfloat16), 'sp', scatter_dimension=...  27.6 us
    all_gather x1, waiting for transfers between devices, shards(): full_back = lax.all_gather(grad_mixed, 'tp', axis=1, tiled=True)  23.7 us
    all_to_all x1, blocking collectives, sum_blocks(): lax.all_to_all(tall.reshape(sp_size, 1, rows, cols), 'sp', split_axis=0,...  16 us
    pallas_call x1, Pallas kernels, row_back(): pl.pallas_call(row_back_kernel, grid=(width // tile,), out_shape=jax.Shap...  10.3 us
    dot_general x1, matrix products, expert_step(): jnp.einsum('rf,rd->fd', back_gate, rows_in, preferred_element_type=jnp.fl...  7.93 us
    dot_general x1, matrix products, expert_step(): jnp.einsum('rf,rd->fd', back_up, rows_in, preferred_element_type=jnp.floa...  7.93 us
  transfers between devices with their start and end apart: 6, of which 5 were waited for; matrix products, arithmetic and copies ran while one was open for 11% of the time, Pallas kernels for 25%

profile of v1, /device:TPU:0, one launch (start us, length us, event | category | flops | bytes accessed | tf_op | source)
XLA Modules:
  0.0 300.5 jit_solution(3956854586350003306)
XLA Ops:
  7.2 0.9 select_reduce_fusion
  8.0 0.6 copy.57
  8.6 5.2 %all-to-all-start = ((f32[4,1,256]{2,1,0:T(1,128)}), f32[4,1,256]{2,1,0:T(1,128)S(1)}, u32[]{:S(2)}, u32[]{:S(2)}) async-start(f32[4,1,256]{2,1,0:T(1,128)} %copy.57), calls=%async_computation | async-start | bytes 8192 | tf_op jit(solution)/shard_map/all_to_all | solution.py:270
  13.8 75.0 %gather_all.1 = (bf16[1024,4096]{1,0:T(8,128)(2,1)}, bf16[1024,4096]{1,0:T(8,128)(2,1)}) custom-call(bf16[256,512]{1,0:T(8,128)(2,1)} %cot_in.1, bf16[256,512]{1,0:T(8,128)(2,1)} %state_in.1), custom_call_target="tpu_custom_call" | custom-call | tf_op jit(solution)/shard_map/gather_all/pallas_call | solution.py:224
  88.8 6.5 %fusion.14 = f32[1024,256]{1,0:T(8,128)S(1)} fusion(bf16[1024,4096]{1,0:T(8,128)(2,1)} %get-tuple-element.15, bf16[1,256,4096]{2,1,0:T(8,128)(2,1)} %param.20), kind=kOutput, calls=%fused_computation.40 | convolution fusion | flops 2147483648 | bytes 11534336 | tf_op jit(solution)/shard_map/rd,fd->rf/dot_general | solution.py:45
  95.3 0.4 copy-done.10
  95.8 3.3 %fusion.16 = f32[1024,256]{1,0:T(8,128)} fusion(bf16[1024,4096]{1,0:T(8,128)(2,1)S(1)} %copy-done.1, bf16[1,256,4096]{2,1,0:T(8,128)(2,1)S(1)} %copy-done.10), kind=kOutput, calls=%fused_computation.42 | convolution fusion | flops 2147483648 | bytes 11534336 | tf_op jit(solution)/shard_map/rd,fd->rf/dot_general | solution.py:46
  99.1 7.2 %multiply_convert_fusion.4 = (bf16[1024,256]{1,0:T(8,128)(2,1)}, bf16[1024,256]{1,0:T(8,128)(2,1)}) fusion(f32[1024,256]{1,0:T(8,128)S(1)} %fusion.14, f32[1024,256]{1,0:T(8,128)} %fusion.16, bf16[1,256,4096]{2,1,0:T(8,128)(2,1)S(1)} %copy-done, bf16[1024,4096]{1,0:T(8,128)(2,1)} %get-tuple-element.14, f32[1024]{0:T(1024)S(1)} %bitcast.53), kind=kOutput, calls=%fused_computation.8 | convolution fusion | flops 2163474432 | bytes 13635584 | tf_op jit(solution)/shard_map/rd,fd->rf/dot_general | solution.py:50
  106.4 10.3 %row_back.1 = bf16[1024,4096]{1,0:T(8,128)(2,1)} custom-call(bf16[1024,256]{1,0:T(8,128)(2,1)} %get-tuple-element.57.gate_ref, bf16[1024,256]{1,0:T(8,128)(2,1)} %get-tuple-element.56.up_ref, bf16[256,4096]{1,0:T(8,128)(2,1)} %bitcast.57, bf16[256,4096]{1,0:T(8,128)(2,1)} %bitcast.58), custom_call_target="tpu_custom_call" | custom-call | flops 4294967296 | bytes 13631488 | tf_op jit(solution)/shard_map/row_back/pallas_call | solution.py:29
  116.7 0.2 all-gather.2.cloned.1.call-start
  117.0 0.8 copy-done.5
  117.7 7.9 %fusion.23 = f32[256,4096]{1,0:T(8,128)} fusion(bf16[1024,256]{1,0:T(8,128)(2,1)S(1)} %copy-done.5, bf16[1024,4096]{1,0:T(8,128)(2,1)} %get-tuple-element.15), kind=kOutput, calls=%fused_computation.47 | convolution fusion | flops 2147483648 | bytes 13107200 | tf_op jit(solution)/shard_map/rf,rd->fd/dot_general | solution.py:57
  125.7 7.9 %fusion.22 = f32[256,4096]{1,0:T(8,128)} fusion(bf16[1024,256]{1,0:T(8,128)(2,1)S(1)} %copy-done.4, bf16[1024,4096]{1,0:T(8,128)(2,1)} %get-tuple-element.15), kind=kOutput, calls=%fused_computation.46 | convolution fusion | flops 2147483648 | bytes 13107200 | tf_op jit(solution)/shard_map/rf,rd->fd/dot_general | solution.py:56
  133.7 5.0 %fusion = f32[256,4096]{1,0:T(8,128)} fusion(bf16[1024,4096]{1,0:T(8,128)(2,1)S(1)} %bitcast.56, f32[1024]{0:T(1024)S(1)} %bitcast.54, f32[1024,256]{1,0:T(8,128)S(1)} %copy-done.13, f32[1024,256]{1,0:T(8,128)S(1)} %copy-done.12), kind=kOutput, calls=%fused_computation.2 | convolution fusion | flops 2161639424 | bytes 14684160 | tf_op jit(solution)/shard_map/rf,rd->fd/dot_general | solution.py:55
  138.6 68.0 %reduce-scatter.3.cloned.1.call-done = bf16[1024,512]{1,0:T(8,128)(2,1)} async-done(((bf16[1024,4096]{1,0:T(8,128)(2,1)}), bf16[1024,512]{1,0:T(8,128)(2,1)}) %reduce-scatter.3.cloned.1.call-update) | async-done | bytes 1048592 | tf_op jit(solution)/shard_map/reduce_scatter | solution.py:278
  206.7 16.0 %all_to_all.14 = bf16[4,1,256,512]{3,2,1,0:T(8,128)(2,1)S(1)} all-to-all(bf16[4,1,256,512]{3,2,1,0:T(8,128)(2,1)} %bitcast.45), channel_id=1, replica_groups=mesh['sp'=4,'tp'=8] {'sp'}, dimensions={0} | all-to-all | bytes 2097152 | tf_op jit(solution)/shard_map/all_to_all | solution.py:240
  222.7 0.1 convert_reduce_fusion
  222.8 0.8 add_convert_fusion
  223.7 0.1 copy.60
  224.0 2.8 collective-permute-start
  226.9 1.2 collective-permute-done
  228.2 23.7 %all-gather.2.cloned.1.call-done = bf16[256,4096]{1,0:T(8,128)(2,1)} async-done(((bf16[256,512]{1,0:T(8,128)(2,1)}), bf16[256,4096]{1,0:T(8,128)(2,1)}) %all-gather.2.cloned.1.call-update) | async-done | bytes 2097168 | tf_op jit(solution)/shard_map/all_gather | solution.py:342
  251.9 3.1 %multiply_convert_fusion.9 = (bf16[256,256]{0,1:T(8,128)(2,1)S(1)}, f32[256,256]{0,1:T(8,128)S(1)}, f32[256,256]{0,1:T(8,128)S(1)}) fusion(f32[256,258]{0,1:T(8,128)S(1)} %convert_multiply_fusion.2, f32[256]{0:T(256)S(1)} %bitcast.49, f32[256]{0:T(256)S(1)} %bitcast.51, f32[256]{0:T(256)S(1)} %bitcast.47, bf16[256,256]{0,1:T(8,128)(2,1)S(1)} %copy.59, ...), kind=kOutput, calls=%fused_computation.32 | convolution fusion | flops 537460736 | bytes 5770240 | tf_op jit(solution)/shard_map/cd,td->ct/dot_general | solution.py:343
  255.0 2.1 convolution_convert_fusion
  257.1 1.3 collective-permute-start.1
  258.4 0.8 copy.66
  259.2 3.4 %collective-permute-done.1 = f32[256,2]{0,1:T(2,128)S(1)} collective-permute-done((f32[256,2]{0,1:T(2,128)S(1)}, f32[256,2]{0,1:T(2,128)S(1)}, u32[]{:S(2)}, u32[]{:S(2)}) %collective-permute-start.1) | collective-permute-done | bytes 2080 | tf_op jit(solution)/shard_map/ppermute | solution.py:14
  262.6 0.1 multiply_convert_fusion.7
  262.7 0.8 copy.68
  263.5 0.8 copy.67
  264.2 27.6 %reduce-scatter.5.cloned.1.call-done = bf16[256,1024]{1,0:T(8,128)(2,1)} async-done(((bf16[256,4096]{1,0:T(8,128)(2,1)}), bf16[256,1024]{1,0:T(8,128)(2,1)}) %reduce-scatter.5.cloned.1.call-update) | async-done | bytes 524304 | tf_op jit(solution)/shard_map/reduce_scatter | solution.py:345
  291.8 2.1 convert_element_type.71
  (46 shorter events, 0.5 us)
Async XLA Ops:
  7.2 92.0 %copy-start = (bf16[1,256,4096]{2,1,0:T(8,128)(2,1)S(1)}, bf16[1,256,4096]{2,1,0:T(8,128)(2,1)}, u32[]{:S(2)}) copy-start(bf16[1,256,4096]{2,1,0:T(8,128)(2,1)} %param.22) | copy-start | bytes 6291460
  8.6 90.5 %all-to-all-start = ((f32[4,1,256]{2,1,0:T(1,128)}), f32[4,1,256]{2,1,0:T(1,128)S(1)}, u32[]{:S(2)}, u32[]{:S(2)}) async-start(f32[4,1,256]{2,1,0:T(1,128)} %copy.57), calls=%async_computation | async-start | bytes 8192 | tf_op jit(solution)/shard_map/all_to_all | solution.py:270
  13.8 192.8 %reduce-scatter.3.cloned.1.call-start = ((), (), s32[]{:S(2)}) async-start(), calls=%async_computation.4 | async-start | bytes 9437184 | tf_op jit(solution)/shard_map/reduce_scatter | solution.py:278
  88.8 6.5 %copy-start.1 = (bf16[1024,4096]{1,0:T(8,128)(2,1)S(1)}, bf16[1024,4096]{1,0:T(8,128)(2,1)}, u32[]{:S(2)}) copy-start(bf16[1024,4096]{1,0:T(8,128)(2,1)} %get-tuple-element.15) | copy-start | bytes 25165828
  88.8 7.0 %copy-start.10 = (bf16[1,256,4096]{2,1,0:T(8,128)(2,1)S(1)}, bf16[1,256,4096]{2,1,0:T(8,128)(2,1)}, u32[]{:S(2)}) copy-start(bf16[1,256,4096]{2,1,0:T(8,128)(2,1)} %param.21) | copy-start | bytes 6291460
  95.8 3.4 %copy-start.11 = (f32[1024,256]{1,0:T(8,128)}, f32[1024,256]{1,0:T(8,128)S(1)}, u32[]{:S(2)}) copy-start(f32[1024,256]{1,0:T(8,128)S(1)} %fusion.14) | copy-start | bytes 3145732
  116.7 1.0 copy-start.5
  116.7 8.9 %copy-start.4 = (bf16[1024,256]{1,0:T(8,128)(2,1)S(1)}, bf16[1024,256]{1,0:T(8,128)(2,1)}, u32[]{:S(2)}) copy-start(bf16[1024,256]{1,0:T(8,128)(2,1)} %get-tuple-element.57.gate_ref) | copy-start | bytes 1572868
  116.7 135.1 %all-gather.2.cloned.1.call-start = ((), (), s32[]{:S(2)}) async-start(), calls=%async_computation.5 | async-start | bytes 2359296 | tf_op jit(solution)/shard_map/all_gather | solution.py:342
  117.7 15.9 %slice-start = ((s8[8388608]{0:T(1024)(128)(4,1)}), s8[4194304]{0:T(1024)(128)(4,1)S(1)}, s32[]{:S(2)}) async-start(s8[8388608]{0:T(1024)(128)(4,1)} %bitcast.55), calls=%async_computation.7 | async-start | bytes 8388608
  125.7 7.9 %slice-start.1 = ((s8[8388608]{0:T(1024)(128)(4,1)}), s8[4194304]{0:T(1024)(128)(4,1)S(1)}, s32[]{:S(2)}) async-start(s8[8388608]{0:T(1024)(128)(4,1)} %bitcast.55), calls=%async_computation.8 | async-start | bytes 8388608
  125.7 7.9 %copy-start.12 = (f32[1024,256]{1,0:T(8,128)S(1)}, f32[1024,256]{1,0:T(8,128)}, u32[]{:S(2)}) copy-start(f32[1024,256]{1,0:T(8,128)} %copy-done.11) | copy-start | bytes 3145732
  125.7 8.0 %copy-start.13 = (f32[1024,256]{1,0:T(8,128)S(1)}, f32[1024,256]{1,0:T(8,128)}, u32[]{:S(2)}) copy-start(f32[1024,256]{1,0:T(8,128)} %fusion.16) | copy-start | bytes 3145732
  133.6 89.2 %copy-start.3 = (bf16[256,512]{1,0:T(8,128)(2,1)S(1)}, bf16[256,512]{1,0:T(8,128)(2,1)}, u32[]{:S(2)}) copy-start(bf16[256,512]{1,0:T(8,128)(2,1)} %cot_in.1) | copy-start | bytes 786436
  138.6 85.1 %copy-start.6 = (bf16[256,256]{1,0:T(8,128)(2,1)S(1)}, bf16[256,256]{1,0:T(8,128)(2,1)}, u32[]{:S(2)}) copy-start(bf16[256,256]{1,0:T(8,128)(2,1)} %param.13) | copy-start | bytes 393220
  138.6 85.2 %copy-start.7 = (bf16[256,256]{1,0:T(8,128)(2,1)S(1)}, bf16[256,256]{1,0:T(8,128)(2,1)}, u32[]{:S(2)}) copy-start(bf16[256,256]{1,0:T(8,128)(2,1)} %param.14) | copy-start | bytes 393220
  138.6 88.2 %copy-start.9 = (f32[3,256]{1,0:T(4,128)S(1)}, f32[3,256]{1,0:T(4,128)}, u32[]{:S(2)}) copy-start(f32[3,256]{1,0:T(4,128)} %param.15) | copy-start | bytes 9220
  138.6 88.2 %copy-start.8 = (bf16[256,256]{1,0:T(8,128)(2,1)S(1)}, bf16[256,256]{1,0:T(8,128)(2,1)}, u32[]{:S(2)}) copy-start(bf16[256,256]{1,0:T(8,128)(2,1)} %param.12) | copy-start | bytes 393220
  223.6 68.2 %reduce-scatter.5.cloned.1.call-start = ((), (), s32[]{:S(2)}) async-start(), calls=%async_computation.6 | async-start | bytes 2621440 | tf_op jit(solution)/shard_map/reduce_scatter | solution.py:345
  224.0 4.1 %collective-permute-start = (bf16[2,256,2]{1,2,0:T(2,128)(2,1)S(1)}, bf16[2,256,2]{1,2,0:T(2,128)(2,1)S(1)}, u32[]{:S(2)}, u32[]{:S(2)}) collective-permute-start(bf16[2,256,2]{1,2,0:T(2,128)(2,1)S(1)} %pad_maximum_fusion.1), channel_id=1, source_target_pairs={{0,8},{8,16},{16,24},{1,9},{9,17},{17,25},{2,10},{10,18},{18,26},{... | collective-permute-start | bytes 6152 | tf_op jit(solution)/shard_map/ppermute | solution.py:14
  251.8 3.1 %copy-start.2 = (bf16[256,4096]{1,0:T(8,128)(2,1)S(1)}, bf16[256,4096]{1,0:T(8,128)(2,1)}, u32[]{:S(2)}) copy-start(bf16[256,4096]{1,0:T(8,128)(2,1)} %all-gather.2.cloned.1.call-done) | copy-start | bytes 6291460
  257.1 5.5 %collective-permute-start.1 = (f32[256,2]{0,1:T(2,128)S(1)}, f32[256,2]{0,1:T(2,128)S(1)}, u32[]{:S(2)}, u32[]{:S(2)}) collective-permute-start(f32[256,2]{0,1:T(2,128)S(1)} %slice.62), channel_id=1, source_target_pairs={{8,0},{16,8},{24,16},{9,1},{17,9},{25,17},{10,2},{18,10},{26,18},{... | collective-permute-start | bytes 6152 | tf_op jit(solution)/shard_map/ppermute | solution.py:14
Sparse Core Ops, SparseCore 0:
  116.8 89.7 reduce-scatter.2
  223.8 28.0 all-gather.1
  257.2 34.5 reduce-scatter.4
